TPU v7x, 512 devices: a whole 4x4x16 slice. The times are simulated.
512 devices in a mesh: dp: 4 (over x), kv: 64 (over z, y), tp: 2 (over core).
Axes of the slice: x: 4, y: 4, z: 16, core: 2. Of those that a mesh axis runs over, the one named last changes fastest.
Arguments:
- tokens: bfloat16 [512, 4096], P('dp', 'kv'), parts along dimension 0, may hold values from -16 to 16
- gain_mix: float32 [4096], P('kv'), may hold values from 0.1 to 1.9
- w_query: bfloat16 [4096, 2048], P('kv', 'tp'), may hold values from -0.09375 to 0.09375
- w_key: bfloat16 [4096, 2048], P('kv', 'tp'), may hold values from -0.09375 to 0.09375
- w_value: bfloat16 [4096, 2048], P('kv', 'tp'), may hold values from -0.09375 to 0.09375
- w_igate: bfloat16 [4096, 16], P('kv', 'tp'), may hold values from -0.09375 to 0.09375
- w_fgate: bfloat16 [4096, 16], P('kv', 'tp'), may hold values from -0.09375 to 0.09375
- bias_igate: float32 [16], P('tp'), may hold values from -1 to 1
- bias_fgate: float32 [16], P('tp'), may hold values from -1 to 4
- memory: float32 [512, 16, 128, 128], P(('dp', 'kv'), 'tp'), parts along dimension 0, may hold values from -0.8 to 0.8
- normalizer: float32 [512, 16, 128], P(('dp', 'kv'), 'tp'), parts along dimension 0, may hold values from -0.8 to 0.8
- stabilizer: float32 [512, 16], P(('dp', 'kv'), 'tp'), parts along dimension 0, may hold values from -1.5 to 1.5
- w_output: bfloat16 [2048, 4096], P('tp', 'kv'), may hold values from -0.125 to 0.125
- gain_mlp: float32 [4096], replicated, may hold values from 0.1 to 1.9
- w_gate: bfloat16 [4096, 11264], P(None, ('kv', 'tp')), may hold values from -0.09375 to 0.09375
- w_up: bfloat16 [4096, 11264], P(None, ('kv', 'tp')), may hold values from -0.09375 to 0.09375
- w_down: bfloat16 [11264, 4096], P(('kv', 'tp')), may hold values from -0.21875 to 0.21875
Outputs:
- mixed: bfloat16 [512, 4096], P('dp', ('kv', 'tp')), parts along dimension 0
- memory_next: float32 [512, 16, 128, 128], P(('dp', 'kv'), 'tp'), parts along dimension 0
- normalizer_next: float32 [512, 16, 128], P(('dp', 'kv'), 'tp'), parts along dimension 0
- stabilizer_next: float32 [512, 16], P(('dp', 'kv'), 'tp'), parts along dimension 0
There are 4 independent parts, one for each index of `dp`. A program takes and returns all parts, laid end to end along the dimension named above; an argument that names none is the same for every part. Nothing has to cross between parts.
All inputs are finite; a program needn't handle non-finite values.
Results may differ from a plain program's by a relative error of at most 0.014.
Values may be sent and summed in bfloat16 or wider, within the bound.
A program may use at most 64 MiB of HBM per device.

v0:
```python
import jax
import jax.numpy as jnp
from jax import lax
from jax.sharding import Mesh
from jax.sharding import PartitionSpec as P

D = 4096
KV = ("kv_0", "kv_1")
DP_KV = ("dp", "kv_0", "kv_1")
KV_TP = ("kv_0", "kv_1", "tp")


epsilon = 1e-06


def gathered_by_axis(x, axes, dim):
    for axis in reversed(axes):
        x = lax.all_gather(x, axis, axis=dim, tiled=True)
    return x


def in_blocks(x, dim, peers):
    shape = x.shape
    tiles = x.reshape(*shape[:dim], peers, shape[dim] // peers, *shape[dim + 1 :])
    return jnp.moveaxis(tiles, dim, 0)


def summed_on_arrival(x, axis, dim):
    tiles = in_blocks(x, dim, lax.axis_size(axis))
    arrived = lax.all_to_all(tiles, axis, split_axis=0, concat_axis=0, tiled=True)
    return arrived.astype(jnp.float32).sum(axis=0)


def in_one_piece(arrays, axis, dim, along):
    columns = [a.reshape(*a.shape[:along], -1) for a in arrays]
    both = jnp.concatenate(columns, axis=along)
    filled, at, gathered = (summed_on_arrival(both, axis, dim), 0, [])
    for a, column in zip(arrays, columns):
        piece = filled[..., at : at + column.shape[along]]
        gathered.append(piece.reshape(*piece.shape[:along], *a.shape[along:]))
        at += column.shape[along]
    return tuple(gathered)


def joined_along(tiles, dim):
    shape = list(tiles.shape[1:])
    shape[dim] *= tiles.shape[0]
    return jnp.moveaxis(tiles, 0, dim).reshape(shape)


def sent_to_all(x, axis):
    copies = jnp.broadcast_to(x, (lax.axis_size(axis), *x.shape))
    return lax.all_to_all(copies, axis, split_axis=0, concat_axis=0, tiled=True)


def gathered_copies(x, axis, dim):
    return joined_along(sent_to_all(x, axis), dim)


def over_copies(x, axis):
    everything = sent_to_all(x, axis)
    return jnp.sum(everything.astype(jnp.float32), axis=0)


def swapped(x, axis, bit):
    return lax.ppermute(x, axis, [(i, i ^ 1 << bit) for i in range(lax.axis_size(axis))])


def cell_update(
    queries, key_proj, values, in_gate, log_forget, memory, normalizer, stabilizer, head_count
):
    batch_rows = queries.shape[0]
    query_heads = queries.astype(jnp.float32).reshape(batch_rows, head_count, -1)
    head_dim = query_heads.shape[2]
    key_heads = key_proj.astype(jnp.float32).reshape(
        batch_rows, head_count, head_dim
    ) * head_dim ** (-0.5)
    value_heads = values.astype(jnp.float32).reshape(batch_rows, head_count, head_dim)
    stab_next = jnp.maximum(stabilizer + log_forget, in_gate)
    keeping = jnp.exp(stabilizer + log_forget - stab_next)
    fresh_weight = jnp.exp(in_gate - stab_next)
    memory_next = (
        keeping[:, :, None, None] * memory
        + fresh_weight[:, :, None, None] * value_heads[:, :, :, None] * key_heads[:, :, None, :]
    )
    norm_next = keeping[:, :, None] * normalizer + fresh_weight[:, :, None] * key_heads
    numerator = jnp.einsum(
        "bhvk,bhk->bhv", memory_next, query_heads, precision=lax.Precision.HIGHEST
    )
    denominator = jnp.einsum("bhk,bhk->bh", norm_next, query_heads, precision=lax.Precision.HIGHEST)
    denominator = jnp.maximum(jnp.abs(denominator), jnp.exp(-stab_next))
    hidden = (numerator / denominator[:, :, None]).reshape(batch_rows, -1).astype(jnp.bfloat16)
    return (hidden, memory_next, norm_next, stab_next)


def mixer_block(residual, gain_mlp, w_gate, w_up, w_down, lower_rows, upper_rows):
    full_rows = gathered_by_axis(residual, KV, 1).astype(jnp.float32)
    scaling = lax.rsqrt(jnp.mean(full_rows * full_rows, axis=1, keepdims=True) + epsilon)
    normed = (full_rows * scaling * gain_mlp).astype(jnp.bfloat16)
    gate_act = jnp.dot(normed, w_gate, preferred_element_type=jnp.float32)
    up_act = jnp.dot(normed, w_up, preferred_element_type=jnp.float32)
    activated = (jax.nn.silu(gate_act) * up_act).astype(jnp.bfloat16)
    paired_units = lax.all_to_all(activated, "tp", split_axis=0, concat_axis=1, tiled=True)
    width = w_down.shape[0]
    down_terms = jnp.dot(paired_units[:, :width], lower_rows, preferred_element_type=jnp.float32)
    down_terms = down_terms + jnp.dot(
        paired_units[:, width:], upper_rows, preferred_element_type=jnp.float32
    )
    half_sums = summed_on_arrival(down_terms.astype(jnp.bfloat16), KV, 1)
    return lax.all_to_all(half_sums, "tp", split_axis=1, concat_axis=0, tiled=True)


def local(
    tokens,
    gain_mix,
    w_query,
    w_key,
    w_value,
    w_igate,
    w_fgate,
    bias_igate,
    bias_fgate,
    memory,
    normalizer,
    stabilizer,
    w_output,
    gain_mlp,
    w_gate,
    w_up,
    w_down,
):
    tok_float = tokens.astype(jnp.float32)
    scaled = (tok_float * gain_mix).astype(jnp.bfloat16)
    part_squares = jnp.sum(tok_float * tok_float, axis=1)
    query_part = jnp.dot(scaled, w_query, preferred_element_type=jnp.float32)
    key_part = jnp.dot(scaled, w_key, preferred_element_type=jnp.float32)
    value_part = jnp.dot(scaled, w_value, preferred_element_type=jnp.float32)
    igate_part = jnp.dot(scaled, w_igate, preferred_element_type=jnp.float32)
    fgate_part = jnp.dot(scaled, w_fgate, preferred_element_type=jnp.float32)
    query_sum, key_sum, value_sum, igate_sum, fgate_sum, own_squares = in_one_piece(
        (
            query_part.astype(jnp.bfloat16),
            key_part.astype(jnp.bfloat16),
            value_part.astype(jnp.bfloat16),
            igate_part.astype(jnp.bfloat16),
            fgate_part.astype(jnp.bfloat16),
            part_squares.astype(jnp.bfloat16),
        ),
        KV,
        0,
        1,
    )
    scaling = lax.rsqrt(own_squares / D + epsilon)[:, None]
    queries = (scaling * query_sum).astype(jnp.bfloat16)
    key_proj = (scaling * key_sum).astype(jnp.bfloat16)
    values = (scaling * value_sum).astype(jnp.bfloat16)
    in_gate = scaling * igate_sum + bias_igate
    log_forget = jax.nn.log_sigmoid(scaling * fgate_sum + bias_fgate)
    hidden, memory_next, norm_next, stab_next = cell_update(
        queries,
        key_proj,
        values,
        in_gate,
        log_forget,
        memory,
        normalizer,
        stabilizer,
        memory.shape[1],
    )
    branch_part = jnp.dot(
        gathered_copies(hidden, KV, 0), w_output, preferred_element_type=jnp.float32
    )
    branch = over_copies(branch_part.astype(jnp.bfloat16), "tp").astype(jnp.float32)
    residual = (tok_float + branch).astype(jnp.bfloat16)
    partner_rows = swapped(w_down, "tp", 0)
    first_core = lax.axis_index("tp") == 0
    lower_rows = jnp.where(first_core, w_down, partner_rows)
    upper_rows = jnp.where(first_core, partner_rows, w_down)
    mixed_terms = mixer_block(residual, gain_mlp, w_gate, w_up, w_down, lower_rows, upper_rows)
    columns = mixed_terms.shape[1]
    residual_own = lax.dynamic_slice_in_dim(residual, lax.axis_index("tp") * columns, columns, 1)
    mixed = (residual_own.astype(jnp.float32) + mixed_terms).astype(jnp.bfloat16)
    return (mixed, memory_next, norm_next, stab_next)


def solution(mesh):
    torus = Mesh(
        mesh.devices.reshape(mesh.shape["dp"], 16, 4, mesh.shape["tp"]),
        ("dp", "kv_0", "kv_1", "tp"),
    )
    in_specs = (
        P("dp", KV),
        P(KV),
        P(KV, "tp"),
        P(KV, "tp"),
        P(KV, "tp"),
        P(KV, "tp"),
        P(KV, "tp"),
        P("tp"),
        P("tp"),
        P(DP_KV, "tp", None, None),
        P(DP_KV, "tp", None),
        P(DP_KV, "tp"),
        P("tp", KV),
        P(),
        P(None, KV_TP),
        P(None, KV_TP),
        P(KV_TP, None),
    )
    out_specs = (P("dp", KV_TP), P(DP_KV, "tp", None, None), P(DP_KV, "tp", None), P(DP_KV, "tp"))
    return jax.shard_map(local, mesh=torus, in_specs=in_specs, out_specs=out_specs, check_vma=False)
```

profile of v0, /device:TPU:1, one launch (start us, length us, event | category | flops | bytes accessed | tf_op | source)
XLA Modules:
  0.0 260.0 jit_solution(14487738798445464333)
XLA Ops:
  7.3 0.8 fusion.14
  8.1 1.2 convolution_convert_fusion.2
  9.5 1.3 convolution_convert_fusion.1
  12.2 1.9 concatenate.19
  14.2 61.4 %all_to_all.58 = bf16[64,2,3089]{2,1,0:T(2,128)(2,1)S(1)} all-to-all(bf16[64,2,3089]{2,1,0:T(2,128)(2,1)S(1)} %concatenate.19), channel_id=1, replica_groups=mesh['dp'=4,'kv_0'=16,'kv_1'=4,'tp'=2] {'kv_0','kv_1'}, dimensions={0} | all-to-all | bytes 1581568 | tf_op jit(solution)/shard_map/all_to_all | solution.py:30
  76.7 0.7 multiply_reduce_fusion
  77.8 1.0 copy-done.1
  78.8 0.9 fusion.40
  80.0 27.5 %all_to_all.59 = bf16[64,2,1024]{2,1,0:T(2,128)(2,1)S(1)} all-to-all(bf16[64,2,1024]{2,1,0:T(2,128)(2,1)S(1)} %broadcast_in_dim.4), channel_id=1, replica_groups=mesh['dp'=4,'kv_0'=16,'kv_1'=4,'tp'=2] {'kv_0','kv_1'}, dimensions={0} | all-to-all | bytes 524288 | tf_op jit(solution)/shard_map/all_to_all | solution.py:53
  107.8 7.9 %all_to_all.60 = bf16[2,128,64]{1,2,0:T(8,128)(2,1)S(1)} all-to-all(bf16[2,128,64]{1,2,0:T(8,128)(2,1)S(1)} %broadcast_in_dim.5), channel_id=1, replica_groups=mesh['dp'=4,'kv_0'=16,'kv_1'=4,'tp'=2] {'tp'}, dimensions={0} | all-to-all | bytes 65536 | tf_op jit(solution)/shard_map/all_to_all | solution.py:53
  115.8 9.7 %all_gather.6 = bf16[128,256]{0,1:T(8,128)(2,1)} all-gather(bf16[128,64]{0,1:T(8,128)(2,1)S(1)} %fusion.15), channel_id=1, replica_groups=mesh['dp'=4,'kv_0'=16,'kv_1'=4,'tp'=2] {'kv_1'}, dimensions={1}, use_global_device_ids=true | all-gather | bytes 81920 | tf_op jit(solution)/shard_map/all_gather | solution.py:18
  125.5 5.1 %collective-permute-start = (bf16[88,4096]{1,0:T(8,128)(2,1)S(1)}, bf16[88,4096]{1,0:T(8,128)(2,1)S(1)}, u32[]{:S(2)}, u32[]{:S(2)}) collective-permute-start(bf16[88,4096]{1,0:T(8,128)(2,1)S(1)} %copy-done.2), channel_id=1, source_target_pairs={{0,1},{1,0},{2,3},{3,2},{4,5},{5,4},{6,7},{7,6},{8,9},{9,8},{10,11... | collective-permute-start | bytes 2162696 | tf_op jit(solution)/shard_map/ppermute | solution.py:66
  130.7 48.6 %all-gather.2.cloned.1.call-done = bf16[128,4096]{0,1:T(8,128)(2,1)} async-done(((bf16[128,256]{0,1:T(8,128)(2,1)}), bf16[128,4096]{0,1:T(8,128)(2,1)}) %all-gather.2.cloned.1.call-update) | async-done | bytes 1048592 | tf_op jit(solution)/shard_map/all_gather | solution.py:18
  179.3 1.9 fusion.1
  181.2 0.8 fusion.11
  182.3 0.8 fusion.4
  183.2 14.4 %all_to_all.61 = bf16[2,64,88]{2,1,0:T(8,128)(2,1)S(1)} all-to-all(bf16[2,64,88]{2,1,0:T(8,128)(2,1)S(1)} %bitcast.49), channel_id=1, replica_groups=mesh['dp'=4,'kv_0'=16,'kv_1'=4,'tp'=2] {'tp'}, dimensions={0} | all-to-all | bytes 45056 | tf_op jit(solution)/shard_map/all_to_all | solution.py:103
  198.5 1.1 reshape.88
  199.6 0.7 copy.64
  200.3 1.5 reshape.100
  201.8 11.0 %all-to-all-start.4 = ((bf16[64,2,2048]{2,1,0:T(2,128)(2,1)}), bf16[64,2,2048]{2,1,0:T(2,128)(2,1)S(1)}, u32[]{:S(2)}, u32[]{:S(2)}) async-start(bf16[64,2,2048]{2,1,0:T(2,128)(2,1)} %reshape.100), calls=%async_computation.4 | async-start | bytes 1048576 | tf_op jit(solution)/shard_map/all_to_all | solution.py:30
  212.9 31.0 %all-to-all-done.4 = bf16[64,2,2048]{2,1,0:T(2,128)(2,1)S(1)} async-done(((bf16[64,2,2048]{2,1,0:T(2,128)(2,1)}), bf16[64,2,2048]{2,1,0:T(2,128)(2,1)S(1)}, u32[]{:S(2)}, u32[]{:S(2)}) %all-to-all-start.4) | async-done | bytes 524320 | tf_op jit(solution)/shard_map/all_to_all | solution.py:30
  245.0 6.2 %all_to_all.62 = f32[2,1,2048]{2,1,0:T(1,128)S(1)} all-to-all(f32[2,1,2048]{2,1,0:T(1,128)S(1)} %reshape.102), channel_id=1, replica_groups=mesh['dp'=4,'kv_0'=16,'kv_1'=4,'tp'=2] {'tp'}, dimensions={0} | all-to-all | bytes 32768 | tf_op jit(solution)/shard_map/all_to_all | solution.py:110
  251.6 0.7 reduce.4
  (79 shorter events, 7.3 us)
Async XLA Ops:
  7.2 174.0 %copy-start = (bf16[4096,88]{0,1:T(8,128)(2,1)S(1)}, bf16[4096,88]{0,1:T(8,128)(2,1)}, u32[]{:S(2)}) copy-start(bf16[4096,88]{0,1:T(8,128)(2,1)} %param.31) | copy-start | bytes 2162692
  7.2 3.7 %copy-start.5 = (bf16[128,64]{0,1:T(8,128)(2,1)S(1)}, bf16[128,64]{0,1:T(8,128)(2,1)}, u32[]{:S(2)}) copy-start(bf16[128,64]{0,1:T(8,128)(2,1)} %param.17) | copy-start | bytes 49156
  7.2 3.7 %copy-start.10 = (f32[64]{0:T(128)S(1)}, f32[64]{0:T(128)}, u32[]{:S(2)}) copy-start(f32[64]{0:T(128)} %param.18) | copy-start | bytes 772
  7.2 3.7 %copy-start.7 = (bf16[64,1024]{1,0:T(8,128)(2,1)S(1)}, bf16[64,1024]{1,0:T(8,128)(2,1)}, u32[]{:S(2)}) copy-start(bf16[64,1024]{1,0:T(8,128)(2,1)} %param.21) | copy-start | bytes 393220
  7.2 172.1 %all-gather.2.cloned.1.call-start = ((), (), s32[]{:S(2)}) async-start(), calls=%async_computation.6 | async-start | bytes 1114112 | tf_op jit(solution)/shard_map/all_gather | solution.py:18
  9.5 1.9 copy-start.16
  9.5 2.2 copy-start.17
  14.1 62.5 %copy-start.11 = (f32[2,8]{1,0:T(2,128)S(1)}, f32[2,8]{1,0:T(2,128)}, u32[]{:S(2)}) copy-start(f32[2,8]{1,0:T(2,128)} %param.28) | copy-start | bytes 196
  14.1 62.4 %copy-start.12 = (f32[8]{0:T(128)S(1)}, f32[8]{0:T(128)}, u32[]{:S(2)}) copy-start(f32[8]{0:T(128)} %param.24) | copy-start | bytes 100
  14.1 62.4 %copy-start.13 = (f32[8]{0:T(128)S(1)}, f32[8]{0:T(128)}, u32[]{:S(2)}) copy-start(f32[8]{0:T(128)} %param.25) | copy-start | bytes 100
  14.1 62.6 %copy-start.9 = (f32[2,8,128]{2,1,0:T(8,128)S(1)}, f32[2,8,128]{2,1,0:T(8,128)}, u32[]{:S(2)}) copy-start(f32[2,8,128]{2,1,0:T(8,128)} %param.27) | copy-start | bytes 24580
  14.1 63.2 %copy-start.4 = (f32[2,8,128,128]{3,2,1,0:T(8,128)S(1)}, f32[2,8,128,128]{3,2,1,0:T(8,128)}, u32[]{:S(2)}) copy-start(f32[2,8,128,128]{3,2,1,0:T(8,128)} %param.26) | copy-start | bytes 3145732
  76.7 1.1 copy-start.8
  77.8 1.0 copy-start.1
  78.8 28.8 %copy-start.6 = (bf16[1024,64]{0,1:T(8,128)(2,1)S(1)}, bf16[1024,64]{0,1:T(8,128)(2,1)}, u32[]{:S(2)}) copy-start(bf16[1024,64]{0,1:T(8,128)(2,1)} %param.29) | copy-start | bytes 393220
  79.8 45.7 %copy-start.2 = (bf16[88,4096]{1,0:T(8,128)(2,1)S(1)}, bf16[88,4096]{1,0:T(8,128)(2,1)}, u32[]{:S(2)}) copy-start(bf16[88,4096]{1,0:T(8,128)(2,1)} %param.33) | copy-start | bytes 2162692
  107.6 73.6 %copy-start.15 = (f32[4096]{0:T(1024)S(1)}, f32[4096]{0:T(1024)}, u32[]{:S(2)}) copy-start(f32[4096]{0:T(1024)} %param.30) | copy-start | bytes 49156
  125.5 72.3 %collective-permute-start = (bf16[88,4096]{1,0:T(8,128)(2,1)S(1)}, bf16[88,4096]{1,0:T(8,128)(2,1)S(1)}, u32[]{:S(2)}, u32[]{:S(2)}) collective-permute-start(bf16[88,4096]{1,0:T(8,128)(2,1)S(1)} %copy-done.2), channel_id=1, source_target_pairs={{0,1},{1,0},{2,3},{3,2},{4,5},{5,4},{6,7},{7,6},{8,9},{9,8},{10,11... | collective-permute-start | bytes 2162696 | tf_op jit(solution)/shard_map/ppermute | solution.py:66
  179.3 1.9 copy-start.3
  181.2 1.1 copy-start.14
  201.8 42.0 %all-to-all-start.4 = ((bf16[64,2,2048]{2,1,0:T(2,128)(2,1)}), bf16[64,2,2048]{2,1,0:T(2,128)(2,1)S(1)}, u32[]{:S(2)}, u32[]{:S(2)}) async-start(bf16[64,2,2048]{2,1,0:T(2,128)(2,1)} %reshape.100), calls=%async_computation.4 | async-start | bytes 1048576 | tf_op jit(solution)/shard_map/all_to_all | solution.py:30
Sparse Core Ops, SparseCore 0:
  125.6 53.6 all-gather.1
where the time goes:
time: 261 us; the launch traced here: 260 us
  blocking collectives  127 us (49%)
  waiting for transfers between devices  79.6 us (30%)
  starting transfers between devices  16.2 us (6%)
  between operations  14.5 us (6%)
  local copies, waits for them, and re-layouts  9.46 us (4%)
  matrix products  6.63 us (3%)
  other arithmetic  6.45 us (2%)
    all_to_all x1, blocking collectives, summed_on_arrival(): lax.all_to_all(tiles, axis, split_axis=0, concat_axis=0, tiled=True)  61.4 us
    all_gather x1, waiting for transfers between devices, gathered_by_axis(): x = lax.all_gather(x, axis, axis=dim, tiled=True)  48.6 us
    all_to_all x2, blocking collectives, sent_to_all(): return lax.all_to_all(copies, axis, split_axis=0, concat_axis=0, tiled=True)  35.4 us
    all_to_all x1, waiting for transfers between devices, summed_on_arrival(): lax.all_to_all(tiles, axis, split_axis=0, concat_axis=0, tiled=True)  31 us
    all_to_all x1, blocking collectives, mixer_block(): lax.all_to_all(activated, 'tp', split_axis=0, concat_axis=1, tiled=True)  14.4 us
    all_to_all x1, starting transfers between devices, summed_on_arrival(): lax.all_to_all(tiles, axis, split_axis=0, concat_axis=0, tiled=True)  11 us
    all_gather x1, blocking collectives, gathered_by_axis(): x = lax.all_gather(x, axis, axis=dim, tiled=True)  9.71 us
    all_to_all x1, blocking collectives, mixer_block(): lax.all_to_all(half_sums, 'tp', split_axis=1, concat_axis=0, tiled=True)  6.17 us
  transfers between devices with their start and end apart: 3, of which 2 were waited for; matrix products, arithmetic and copies ran while one was open for 1% of the time, Pallas kernels for 0%

commit v1 on v0

v1 whole, which is shorter than its diff:
```python
import functools

import jax
import jax.numpy as jnp
from jax import lax
from jax.experimental import pallas as pl
from jax.experimental.pallas import tpu as pltpu
from jax.sharding import Mesh
from jax.sharding import PartitionSpec as P

KV = ("kv_0", "kv_1")
DP_KV = ("dp", "kv_0", "kv_1")
KV_TP = ("kv_0", "kv_1", "tp")
MESH = pl.DeviceIdType.MESH
EPS = 1e-06
HD = 128

f32 = jnp.float32
bf16 = jnp.bfloat16


def dot(a, b, dims):
    return lax.dot_general(a, b, (dims, ((), ())), preferred_element_type=f32)


NN = ((1,), (0,))
NT = ((1,), (1,))


def near_first(k, n):
    half, odd = k // 2, k % 2
    return (1 - odd) * (half + 1) + odd * (n - 1 - half)


ORDER = {
    4: (2, 1, 3, 0),
    8: (4, 3, 5, 2, 6, 1, 7, 0),
    16: (8, 7, 9, 6, 10, 5, 11, 4, 12, 3, 13, 2, 14, 1, 15, 0),
}
JOINED = {4: {}, 8: {}, 16: {}}


def layer(
    nz,
    ny,
    tok_hbm,
    gain_hbm,
    wq_hbm,
    wk_hbm,
    wv_hbm,
    wig_hbm,
    wfg_hbm,
    big_hbm,
    bfg_hbm,
    mem_hbm,
    norm_hbm,
    stab_hbm,
    wo_hbm,
    gmlp_hbm,
    wg_hbm,
    wu_hbm,
    wd_hbm,
    mixed_ref,
    memory_ref,
    norm_ref,
    stab_ref,
    tok,
    gain,
    wqkv,
    wig,
    wfg,
    wgate,
    big,
    bfg,
    mem,
    norm,
    stab,
    wo,
    gmlp,
    wraw,
    wfold,
    wdraw,
    wdt,
    memhl,
    ysend,
    yrecv,
    tq,
    zsend,
    zrelay,
    zrecv,
    zgsend,
    zgrecv,
    hidg,
    hidf,
    bsend,
    brecv,
    res,
    resg,
    xsend,
    xrecv,
    dsend,
    drecv,
    esend,
    erelay,
    erecv,
    loc_sem,
    pair_send,
    pair_recv,
    y1_send,
    y1_recv,
    z1_send,
    z1_relay,
    z1_recv,
    z2_send,
    z2_recv,
    y2_send,
    y2_recv,
    z3_send,
    z3_recv,
    y3_send,
    y3_recv,
    y5_send,
    y5_recv,
    z5_send,
    z5_relay,
    z5_recv,
):
    nkv = nz * ny
    rows = 2 * nkv
    hz = nz // 2
    cols = tok.shape[0]
    model = nkv * cols
    khalf = model // 2
    ff = wraw.shape[1]
    fpad = wfold.shape[0] // 4
    own_cols = mixed_ref.shape[0]
    z = lax.axis_index("kv_0")
    y = lax.axis_index("kv_1")
    c = lax.axis_index("tp")
    other = 1 - c

    def zpeer(d):
        return lax.rem(z + d, nz)

    def ypeer(d):
        return lax.rem(y + d, ny)

    def rcopy(src, dst, ssem, rsem, axis, to):
        return pltpu.make_async_remote_copy(
            src_ref=src, dst_ref=dst, send_sem=ssem, recv_sem=rsem, device_id={axis: to}, device_id_type=MESH
        )

    def local(src, dst, k):
        return pltpu.make_async_copy(src, dst, loc_sem.at[k])

    chunk = ny * cols

    def from_z(m, core):
        return pl.ds(pl.multiple_of((2 * m + core) * chunk, 128), chunk)

    def place(m):
        return pl.ds(m * chunk, chunk)

    first = [
        local(tok_hbm, tok, 0),
        local(gain_hbm, gain, 1),
        local(wig_hbm, wig, 2),
        local(wfg_hbm, wfg, 3),
        local(wq_hbm, wqkv.at[0], 4),
        local(wk_hbm, wqkv.at[1], 4),
        local(wv_hbm, wqkv.at[2], 4),
    ]
    small = [local(big_hbm, big, 5), local(bfg_hbm, bfg, 6), local(stab_hbm, stab, 7), local(norm_hbm, norm, 8)]
    memory = local(mem_hbm, mem, 9)
    late = []
    for m in range(hz):
        late += [
            local(gmlp_hbm.at[:, from_z(m, c)], gmlp.at[:, place(m)], 10),
            local(wg_hbm.at[:, from_z(m, c)], wraw.at[2 * c, :, place(m)], 11),
            local(wu_hbm.at[:, from_z(m, c)], wraw.at[2 * c + 1, :, place(m)], 11),
        ]
    down = local(wd_hbm, wdraw.at[c], 12)
    output = local(wo_hbm, wo, 13)
    for op in first:
        op.start()

    barrier = pltpu.get_barrier_semaphore()

    def greet(d, _):
        pl.semaphore_signal(barrier, inc=1, device_id={"kv_0": zpeer(d)}, device_id_type=MESH)
        return 0

    lax.fori_loop(1, nz, greet, 0)
    for d in range(1, ny):
        pl.semaphore_signal(barrier, inc=1, device_id={"kv_1": ypeer(d)}, device_id_type=MESH)
    pl.semaphore_signal(barrier, inc=1, device_id={"tp": other}, device_id_type=MESH)
    for op in small + [memory] + late + [down, output]:
        op.start()

    for op in first[:4]:
        op.wait()
    groups = dsend.shape[1]
    per = nz // groups
    grow = 2 * per
    order = ORDER[nz]
    odds = [o for o in order if o % 2]
    joined = JOINED[nz]
    relayed = sorted(joined.values())
    final = [o for o in order if o and o not in relayed]
    p = lax.broadcasted_iota(jnp.int32, (rows, 1), 0)
    r = lax.broadcasted_iota(jnp.int32, (rows, rows), 1)
    group = p // (ny * grow)
    to_y, to_b, to_i = (p // grow) % ny, (p // per) % 2, p % per
    turn_of = group * per + to_i
    offset = jnp.zeros_like(p)
    for k, o in enumerate(order):
        offset = jnp.where(turn_of == k, o, offset)
    to_z = (z + offset) % nz
    perm = jnp.where(2 * ny * to_z + 2 * to_y + to_b == r, 1.0, 0.0).astype(bf16)
    tokp = dot(perm, tok[...], NT)
    scaled = (tokp * gain[...]).astype(bf16)
    wgate[...] = jnp.zeros_like(wgate)
    wgate[0:8, :] = wig[...].astype(f32)
    wgate[8:16, :] = wfg[...].astype(f32)
    wgate[64:72, :] = wig[...].astype(f32)
    wgate[72:80, :] = wfg[...].astype(f32)
    row_id = lax.broadcasted_iota(jnp.int32, (HD, cols), 0)
    ones = jnp.where((row_id == 16) | (row_id == 80), 1.0, 0.0).astype(bf16)
    squares = tokp * tokp
    sq_hi = squares.astype(bf16)
    sq_lo = (squares - sq_hi.astype(f32)).astype(bf16)
    gates = dot(scaled, wgate[...].astype(bf16), NT) + dot(sq_hi, ones, NT) + dot(sq_lo, ones, NT)

    def in_two(total):
        lane = lax.broadcasted_iota(jnp.int32, total.shape, 1)
        high = total.astype(bf16).astype(f32)
        return jnp.where(lane < 64, high, total - high)

    gates = in_two(gates)
    width = wqkv.shape[2]
    far_first = sorted(range(1, ny), key=lambda d: -min(d, ny - d))

    def y1(g, d):
        return rcopy(
            ysend.at[g, ypeer(d)], yrecv.at[g, d - 1], y1_send.at[0], y1_recv.at[g], "kv_1", ypeer(d)
        )

    pltpu.make_async_copy(wqkv, wqkv, loc_sem.at[4]).wait()
    for g in range(groups):
        part = slice(g * ny * grow, (g + 1) * ny * grow)
        for k in range(4):
            if k < 3:
                values = dot(scaled[part], wqkv[k], NN)
                at = k * width
            else:
                values = gates[part]
                at = 3 * width
            for to in range(ny):
                ysend[g, to, :, at : at + values.shape[1]] = values[to * grow : (to + 1) * grow].astype(bf16)
        if g == 0:
            pl.semaphore_wait(barrier, (nz - 1) + (ny - 1) + 1)
        for d in far_first:
            y1(g, d).start()

    pair = [rcopy(wd_hbm, wdraw.at[c], pair_send.at[1], pair_recv.at[1], "tp", other)]
    for m in range(hz):
        for k, w_hbm in enumerate((wg_hbm, wu_hbm)):
            pair.append(
                rcopy(
                    w_hbm.at[:, from_z(m, other)],
                    wraw.at[2 * c + k, :, place(m)],
                    pair_send.at[0],
                    pair_recv.at[0],
                    "tp",
                    other,
                )
            )
    for op in pair:
        op.start()

    memory.wait()

    def split_memory(i, _):
        m = mem[i]
        high = m.astype(bf16)
        memhl[i, :, 0:HD] = high
        memhl[i, :, HD : 2 * HD] = (m - high.astype(f32)).astype(bf16)
        return 0

    lax.fori_loop(0, mem.shape[0], split_memory, 0)

    zrow = zsend.shape[1]

    def onward(o, send, relay, recv, send_sem, relay_sem, recv_sem):
        if o not in relayed:
            return rcopy(send.at[o], recv.at[o], send_sem, recv_sem, "kv_0", zpeer(o))
        near = 1 if o < nz // 2 else nz - 1
        return rcopy(send.at[o], relay.at[o], send_sem, relay_sem.at[relayed.index(o)], "kv_0", zpeer(near))

    def z1(o):
        return onward(o, zsend, zrelay, zrecv, z1_send.at[0], z1_relay, z1_recv.at[0])

    def zg(o):
        return rcopy(zgsend.at[o], zgrecv.at[o], z1_send.at[1], z1_recv.at[1], "kv_0", zpeer(o))

    def together(ref, sem):
        return pltpu.make_async_copy(ref, ref, sem)

    for g in range(groups):
        together(yrecv.at[g], y1_recv.at[g]).wait()
        for k in range(25):
            part = slice(k * HD, (k + 1) * HD)
            total = ysend[g, y, :, part].astype(f32)
            for d in range(ny - 1):
                total = total + yrecv[g, d, :, part].astype(f32)
            if k < 24:
                for b in range(2):
                    at = g * per * zrow + (k // 8) * 16 + b * 8 + k % 8
                    tq[pl.ds(at, per, stride=zrow), :] = total[b * per : (b + 1) * per]
            else:
                total = total + pltpu.roll(total, 64, 1)
                lane = lax.broadcasted_iota(jnp.int32, (1, HD), 1)
                for i in range(per):
                    o = order[g * per + i]
                    zgsend[o] = jnp.where(lane < 64, total[i : i + 1], total[per + i : per + i + 1])
                    if o:
                        zg(o).start()
        for k in range(g * per, (g + 1) * per):
            o = order[k]
            if o == 0:
                continue
            total = tq[k * zrow : (k + 1) * zrow, :]
            e = joined.get(o)
            if e is not None:
                z1(e).wait_recv()
                total = total + zrelay[e].astype(f32)
            zsend[o] = total.astype(bf16)
            z1(o).start()

    own_pair, far_pair = pl.ds(2 * c, 2), pl.ds(2 * other, 2)
    together(gmlp, loc_sem.at[10]).wait()
    together(wraw.at[own_pair], loc_sem.at[11]).wait()
    together(wraw.at[far_pair], pair_recv.at[0]).wait()
    fold_width = min(256, khalf)
    for t in range(4):
        if fpad > ff:
            wfold[t * fpad + ff : (t + 1) * fpad, :] = jnp.zeros((fpad - ff, khalf), bf16)

    def fold(i, _):
        part = pl.ds(pl.multiple_of(i * fold_width, 128), fold_width)
        for t in range(4):
            wfold[t * fpad : t * fpad + ff, part] = (wraw[t, :, part].astype(f32) * gmlp[:, part]).astype(bf16)
        return 0

    lax.fori_loop(0, khalf // fold_width, fold, 0)
    down.wait()
    pair[0].wait_recv()

    def turn(i, _):
        part = pl.ds(pl.multiple_of(i * HD, 128), HD)
        for t in range(2):
            wdt[t, pl.ds(pl.multiple_of(i * HD, 128), HD), :] = wdraw[t, :, part].astype(f32).T.astype(bf16)
        return 0

    lax.fori_loop(0, model // HD, turn, 0)

    for op in small:
        op.wait()

    sums = tq[order.index(0) * zrow : (order.index(0) + 1) * zrow, :]
    together(zgrecv.at[pl.ds(1, nz - 1)], z1_recv.at[1]).wait()
    gsum = zgsend[0]
    for o in range(1, nz):
        gsum = gsum + zgrecv[o]
    together(zrecv.at[pl.ds(1, len(final))], z1_recv.at[0]).wait()
    sums = tq[order.index(0) * zrow : (order.index(0) + 1) * zrow, :]
    for o in final:
        sums = sums + zrecv[o].astype(f32)
    lane8 = lax.broadcasted_iota(jnp.int32, (8, HD), 1)
    sub8 = lax.broadcasted_iota(jnp.int32, (8, HD), 0)
    eye = lax.broadcasted_iota(jnp.int32, (8, 8), 0) == lax.broadcasted_iota(jnp.int32, (8, 8), 1)

    def column(row):
        return jnp.sum(jnp.where(eye, jnp.broadcast_to(row, (8, 8)), 0.0), axis=1, keepdims=True)

    def picked(row, at):
        return jnp.sum(jnp.where(lane8 == sub8 + at, jnp.broadcast_to(row, (8, HD)), 0.0), axis=1, keepdims=True)

    scales, keeps, freshes, stabs = [], [], [], []
    for b in range(2):
        row = gsum
        square = jnp.sum(jnp.where(lane8 == 64 * b + 16, jnp.broadcast_to(row, (8, HD)), 0.0), axis=1, keepdims=True)
        scale = lax.rsqrt(square / model + EPS)
        in_gate = scale * picked(row, 64 * b) + column(big[...])
        forget = scale * picked(row, 64 * b + 8) + column(bfg[...])
        log_forget = jnp.minimum(forget, 0.0) - jnp.log1p(jnp.exp(-jnp.abs(forget)))
        carried = column(stab[b : b + 1, :]) + log_forget
        stab_next = jnp.maximum(carried, in_gate)
        scales.append(scale)
        keeps.append(jnp.exp(carried - stab_next))
        freshes.append(jnp.exp(in_gate - stab_next))
        stabs.append(stab_next)
    scale = jnp.concatenate(scales, axis=0)
    keep = jnp.concatenate(keeps, axis=0)
    fresh = jnp.concatenate(freshes, axis=0)
    stab_next = jnp.concatenate(stabs, axis=0)

    def arrived(k):
        return (scale * sums[16 * k : 16 * (k + 1)]).astype(bf16)

    query16 = arrived(0)
    query = query16.astype(f32)
    twice = jnp.concatenate([query16, query16], axis=1)
    sub16 = lax.broadcasted_iota(jnp.int32, (16, HD), 0)
    kept = jnp.zeros((16, HD), f32)
    for i in range(16):
        kept = kept + jnp.where(sub16 == i, dot(twice, memhl[i], NT), 0.0)
    key = arrived(1).astype(f32) * HD ** (-0.5)
    old_norm = norm[...]
    norm_next = keep * old_norm + fresh * key
    match = jnp.sum(key * query, axis=1, keepdims=True)
    bottom = jnp.sum(norm_next * query, axis=1, keepdims=True)
    bottom = jnp.maximum(jnp.abs(bottom), jnp.exp(-stab_next))
    value = arrived(2).astype(f32)
    hidden = (keep * kept + (fresh * match) * value) / bottom
    me = z * ny + y
    hidg[me] = hidden.astype(bf16)

    def z2(d):
        return rcopy(hidg.at[me], hidg.at[me], z2_send.at[0], z2_recv.at[d], "kv_0", zpeer(d))

    def z2_in(d):
        j = lax.rem(z + nz - d, nz) * ny + y
        return rcopy(hidg.at[j], hidg.at[j], z2_send.at[0], z2_recv.at[d], "kv_0", zpeer(d))

    def y2(d, dz):
        j = lax.rem(z + nz - dz, nz) * ny + y
        return rcopy(hidg.at[j], hidg.at[j], y2_send.at[0], y2_recv.at[0], "kv_1", ypeer(d))

    def start_z2(i, _):
        z2(near_first(nz - 2 - i, nz)).start()
        return 0

    lax.fori_loop(0, nz - 1, start_z2, 0)
    for d in far_first:
        y2(d, 0).start()

    norm_ref[...] = norm_next
    stab_ref[...] = jnp.concatenate(
        [jnp.sum(jnp.where(eye, jnp.broadcast_to(x, (8, 8)), 0.0), axis=0, keepdims=True) for x in stabs], axis=0
    )
    added = jnp.concatenate([fresh * value, jnp.zeros((HD - 16, HD), f32)], axis=0).T
    for i in range(16):
        memory_ref[i] = keep[i : i + 1, :] * mem[i] + added[:, i : i + 1] * key[i : i + 1, :]

    def forward_z2(i, _):
        dz = near_first(i, nz)
        z2_in(dz).wait_recv()
        for d in far_first:
            y2(d, dz).start()
        return 0

    lax.fori_loop(0, nz - 1, forward_z2, 0)
    output.wait()

    together(hidg.at[pl.ds(0, (ny - 1) * nz)], y2_recv.at[0]).wait()
    hidf[...] = hidg[...].astype(f32).reshape(nkv * 16, HD)
    branch = jnp.zeros((cols, rows), f32)
    for h in range(8):
        head = hidf[pl.ds(h, rows, stride=8), :].astype(bf16)
        branch = branch + dot(wo[:, h * HD : (h + 1) * HD], head, NT)
    bsend[...] = branch.astype(bf16)
    swap_branch = rcopy(bsend, brecv, pair_send.at[2], pair_recv.at[2], "tp", other)
    swap_branch.start()
    swap_branch.wait_recv()
    residual = (tok[...].astype(f32) + (bsend[...].astype(f32) + brecv[...].astype(f32))).astype(bf16)
    res[...] = residual

    zz = z // 2
    odd = lax.rem(z + c, 2)
    mine = odd == 0

    def z3(d):
        return rcopy(res, resg.at[zz, y], z3_send.at[0], z3_recv.at[d], "kv_0", zpeer(d))

    def y3_own(d):
        return rcopy(res, resg.at[zz, y], y3_send.at[0], y3_recv.at[zz], "kv_1", ypeer(d))

    def y3(d, i):
        return rcopy(resg.at[i, y], resg.at[i, y], y3_send.at[0], y3_recv.at[i], "kv_1", ypeer(d))

    @pl.when(mine)
    def _():
        for o in odds:
            z3(o).start()
        for d in far_first:
            y3_own(d).start()
        resg[zz, y] = residual

    def offset3(k):
        step = jnp.maximum(k - 1, 0)
        even = jnp.where(k == 0, 0, 2 * near_first(step, hz))
        uneven = jnp.where(k % 2 == 0, k + 1, nz - k)
        return jnp.where(odd == 0, even, uneven)

    def source3(k):
        return lax.rem(z + nz - offset3(k), nz)

    def z3_in(k):
        at = resg.at[source3(k) // 2, y]
        return rcopy(at, at, z3_send.at[0], z3_recv.at[offset3(k)], "kv_0", source3(k))

    def z3_relay(k):
        at = resg.at[source3(k) // 2, y]
        step = 1 - 2 * lax.rem(k, 2)
        d = offset3(k) + step
        return rcopy(at, at, z3_send.at[0], z3_recv.at[d], "kv_0", lax.rem(z + nz + step, nz))

    def accumulate(i):
        together(resg.at[i, pl.ds(0, ny - 1)], y3_recv.at[i]).wait()
        block = resg[i].reshape(ny * cols, rows)
        part = pl.ds(pl.multiple_of(i * (ny * cols), 128), ny * cols)
        xsend[0 : 4 * fpad, :] += dot(wfold[:, part], block, NN)
        wide = block.astype(f32)
        square = jnp.sum((wide * wide).reshape(ny * cols // 8, 8, rows), axis=0)
        xsend[4 * fpad : 4 * fpad + 8, :] += square

    lag = min(3, hz)
    xsend[...] = jnp.zeros_like(xsend)

    def forward_z3(k):
        @pl.when(jnp.logical_not(mine & (k == 0)))
        def _():
            z3_in(k).wait_recv()

            @pl.when(jnp.logical_not(mine) & (k < hz - 1))
            def _():
                z3_relay(k).start()

            for d in far_first:
                y3(d, source3(k) // 2).start()

    def late_z3(k):
        accumulate(source3(k) // 2)

    def only_forward(k, _):
        forward_z3(k)
        return 0

    def both(k, _):
        forward_z3(k)
        late_z3(k - lag)
        return 0

    def only_late(k, _):
        late_z3(k)
        return 0

    lax.fori_loop(0, lag, only_forward, 0)
    lax.fori_loop(lag, hz, both, 0)
    lax.fori_loop(hz - lag, hz, only_late, 0)
    swap_sums = rcopy(xsend, xrecv, pair_send.at[3], pair_recv.at[3], "tp", other)
    swap_sums.start()
    swap_sums.wait_recv()
    square = jnp.sum(xsend[4 * fpad :, :] + xrecv[4 * fpad :, :], axis=0, keepdims=True)
    scale = lax.rsqrt(square / model + EPS)

    def units(t):
        part = slice(t * fpad, t * fpad + ff)
        return (xsend[part, :] + xrecv[part, :]) * scale

    active = []
    for t in range(2):
        gate, up = units(2 * t), units(2 * t + 1)
        active.append((gate / (1.0 + jnp.exp(-gate)) * up).astype(bf16))

    def y5(d, g):
        return rcopy(dsend.at[ypeer(d), g], drecv.at[g, d - 1], y5_send.at[0], y5_recv.at[g], "kv_1", ypeer(d))

    def place5(k):
        return zpeer(order[k])

    def produce(to, g):
        total = jnp.zeros((per * own_cols, rows), f32)
        for t in range(2):
            parts = [
                wdt[t, pl.ds(pl.multiple_of((place5(g * per + i) * ny + to) * cols + c * own_cols, own_cols), own_cols), :]
                for i in range(per)
            ]
            total = total + dot(jnp.concatenate(parts, axis=0), active[t], NN)
        dsend[to, g] = total.astype(bf16)

    for g in range(groups):
        for d in far_first:
            produce(ypeer(d), g)
            y5(d, g).start()
    for g in range(groups):
        produce(y, g)

    def z5(o):
        return onward(o, esend, erelay, erecv, z5_send.at[0], z5_relay, z5_recv.at[0])

    for g in range(groups):
        together(drecv.at[g], y5_recv.at[g]).wait()
        total = dsend[y, g].astype(f32)
        for d in range(ny - 1):
            total = total + drecv[g, d].astype(f32)
        for i in range(per):
            o = order[g * per + i]
            part = total[i * own_cols : (i + 1) * own_cols]
            if o == 0:
                mixed_sum = part
                continue
            e = joined.get(o)
            if e is not None:
                z5(e).wait_recv()
                part = part + erelay[e].astype(f32)
            esend[o] = part.astype(bf16)
            z5(o).start()

    together(erecv.at[pl.ds(1, len(final))], z5_recv.at[0]).wait()
    for o in final:
        mixed_sum = mixed_sum + erecv[o].astype(f32)
    own_res = res[pl.ds(pl.multiple_of(c * own_cols, own_cols), own_cols), :].astype(f32)
    mixed_ref[...] = (own_res + mixed_sum).astype(bf16)

    for op in [pair[0], swap_branch, swap_sums]:
        op.wait_send()
    together(wraw.at[far_pair], pair_send.at[0]).wait()
    together(yrecv, y1_send.at[0]).wait()
    together(zsend.at[pl.ds(1, nz - 1)], z1_send.at[0]).wait()
    together(zgsend.at[pl.ds(1, nz - 1)], z1_send.at[1]).wait()
    together(hidg.at[pl.ds(0, nz - 1)], z2_send.at[0]).wait()
    together(hidg.at[pl.ds(0, (ny - 1) * nz)], y2_send.at[0]).wait()
    together(drecv, y5_send.at[0]).wait()
    together(esend.at[pl.ds(1, nz - 1)], z5_send.at[0]).wait()
    together(resg.at[:, pl.ds(0, ny - 1)], y3_send.at[0]).wait()

    @pl.when(mine)
    def _():
        together(resg.at[:, 0], z3_send.at[0]).wait()

    @pl.when(jnp.logical_not(mine))
    def _():
        together(resg.at[pl.ds(0, hz - 1), 0], z3_send.at[0]).wait()


def store(mixed, memory, norm, stab, mixed_out, memory_out, norm_out, stab_out, sem):
    pairs = ((memory, memory_out), (norm, norm_out), (stab, stab_out), (mixed, mixed_out))
    copies = [pltpu.make_async_copy(src, dst, sem.at[k]) for k, (src, dst) in enumerate(pairs)]
    for op in copies:
        op.start()
    for op in copies:
        op.wait()


def local(nz, ny, *args):
    (tokens, gain_mix, w_query, w_key, w_value, w_igate, w_fgate, bias_igate, bias_fgate) = args[:9]
    (memory, normalizer, stabilizer, w_output, gain_mlp, w_gate, w_up, w_down) = args[9:]
    rows, cols = tokens.shape
    nkv = nz * ny
    model = nkv * cols
    ff = w_down.shape[0]
    fpad = (ff + 15) // 16 * 16
    heads = memory.shape[1]
    width = heads * HD
    total = HD + 3 * width
    own_cols = cols // 2
    groups = min(4, nz)
    per = nz // groups
    hz = nz // 2
    zrow = 6 * heads
    joins = max(1, len(JOINED[nz]))
    vm = pltpu.VMEM
    dma = pltpu.SemaphoreType.DMA
    operands = (
        tokens.T,
        gain_mix.reshape(1, cols),
        w_query,
        w_key,
        w_value,
        w_igate.T,
        w_fgate.T,
        bias_igate.reshape(1, heads),
        bias_fgate.reshape(1, heads),
        memory.reshape(2 * heads, HD, HD),
        normalizer.reshape(2 * heads, HD),
        stabilizer,
        w_output.T,
        gain_mlp.reshape(1, model),
        w_gate.T,
        w_up.T,
        w_down,
    )
    scratch = [
        vm((cols, rows), bf16),
        vm((1, cols), f32),
        vm((3, cols, width), bf16),
        vm((heads, cols), bf16),
        vm((heads, cols), bf16),
        vm((HD, cols), f32),
        vm((1, heads), f32),
        vm((1, heads), f32),
        vm((2 * heads, HD, HD), f32),
        vm((2 * heads, HD), f32),
        vm((2, heads), f32),
        vm((cols, width), bf16),
        vm((1, model // 2), f32),
        vm((4, ff, model // 2), bf16),
        vm((4 * fpad, model // 2), bf16),
        vm((2, ff, model), bf16),
        vm((2, model, ff), bf16),
        vm((2 * heads, HD, 2 * HD), bf16),
        vm((groups, ny, 2 * per, total), bf16),
        vm((groups, ny - 1, 2 * per, total), bf16),
        vm((nz * zrow, HD), f32),
        vm((nz, zrow, HD), bf16),
        vm((nz, zrow, HD), bf16),
        vm((nz, zrow, HD), bf16),
        vm((nz, 1, HD), f32),
        vm((nz, 1, HD), f32),
        vm((nkv, 2 * heads, HD), bf16),
        vm((nkv * 2 * heads, HD), f32),
        vm((cols, rows), bf16),
        vm((cols, rows), bf16),
        vm((cols, rows), bf16),
        vm((hz, ny, cols, rows), bf16),
        vm((4 * fpad + 8, rows), f32),
        vm((4 * fpad + 8, rows), f32),
        vm((ny, groups, per * own_cols, rows), bf16),
        vm((groups, ny - 1, per * own_cols, rows), bf16),
        vm((nz, own_cols, rows), bf16),
        vm((nz, own_cols, rows), bf16),
        vm((nz, own_cols, rows), bf16),
        dma((14,)),
        dma((4,)),
        dma((4,)),
        dma((1,)),
        dma((groups,)),
        dma((2,)),
        dma((joins,)),
        dma((2,)),
        dma((1,)),
        dma((nz,)),
        dma((1,)),
        dma((1,)),
        dma((1,)),
        dma((nz,)),
        dma((1,)),
        dma((hz,)),
        dma((1,)),
        dma((groups,)),
        dma((1,)),
        dma((joins,)),
        dma((1,)),
    ]
    shapes = (
        ((own_cols, rows), bf16),
        ((2 * heads, HD, HD), f32),
        ((2 * heads, HD), f32),
        ((2, heads), f32),
    )
    held = pl.pallas_call(
        functools.partial(layer, nz, ny),
        out_shape=tuple(vm(*x) for x in shapes),
        in_specs=[pl.BlockSpec(memory_space=pl.ANY)] * len(operands),
        out_specs=tuple(pl.BlockSpec(memory_space=pltpu.VMEM) for _ in shapes),
        scratch_shapes=scratch,
        compiler_params=pltpu.CompilerParams(
            collective_id=0, has_side_effects=True, vmem_limit_bytes=56 * 1024 * 1024
        ),
    )(*operands)
    mixed, memory_next, norm_next, stab_next = pl.pallas_call(
        store,
        out_shape=tuple(jax.ShapeDtypeStruct(*x) for x in shapes),
        in_specs=[pl.BlockSpec(memory_space=pltpu.VMEM) for _ in shapes],
        out_specs=tuple(pl.BlockSpec(memory_space=pl.ANY) for _ in shapes),
        scratch_shapes=[dma((4,))],
    )(*[pltpu.with_memory_space_constraint(x, pltpu.VMEM) for x in held])
    return mixed.T, memory_next.reshape(2, heads, HD, HD), norm_next.reshape(2, heads, HD), stab_next


def solution(mesh):
    dp, nkv, tp = (mesh.shape[a] for a in ("dp", "kv", "tp"))
    ny = 4
    nz = nkv // ny
    torus = Mesh(mesh.devices.reshape(dp, nz, ny, tp), ("dp", "kv_0", "kv_1", "tp"))
    in_specs = (
        P("dp", KV),
        P(KV),
        P(KV, "tp"),
        P(KV, "tp"),
        P(KV, "tp"),
        P(KV, "tp"),
        P(KV, "tp"),
        P("tp"),
        P("tp"),
        P(DP_KV, "tp", None, None),
        P(DP_KV, "tp", None),
        P(DP_KV, "tp"),
        P("tp", KV),
        P(),
        P(None, KV_TP),
        P(None, KV_TP),
        P(KV_TP, None),
    )
    out_specs = (P("dp", KV_TP), P(DP_KV, "tp", None, None), P(DP_KV, "tp", None), P(DP_KV, "tp"))
    return jax.shard_map(
        functools.partial(local, nz, ny), mesh=torus, in_specs=in_specs, out_specs=out_specs, check_vma=False
    )
```

time: 261 us -> 75.8 us (0.29)
  blocking collectives: 127 us -> 0 us
  waiting for transfers between devices: 79.6 us -> 0 us
  Pallas kernels: 0 us -> 75 us
  starting transfers between devices: 16.2 us -> 0 us
  between operations: 14.5 us -> 0.65 us
  local copies, waits for them, and re-layouts: 9.46 us -> 0 us
  matrix products: 6.63 us -> 0 us
  other arithmetic: 6.45 us -> 0 us
    all_to_all x5 -> x0, blocking collectives: 117 us -> none  [the longest x1 61.4 us: summed_on_arrival(): lax.all_to_all(tiles, axis, split_axis=0, concat_axis=0, tiled=True)]
    pallas_call x0 -> x2, Pallas kernels: none -> 75 us  [the longest x1 74 us: local(): pl.pallas_call(functools.partial(layer, nz, ny), out_shape=tuple((vm(*x)...]
    all_gather x1 -> x0, waiting for transfers between devices: 48.6 us -> none  [gathered_by_axis(): x = lax.all_gather(x, axis, axis=dim, tiled=True)]
    all_to_all x1 -> x0, waiting for transfers between devices: 31 us -> none  [summed_on_arrival(): lax.all_to_all(tiles, axis, split_axis=0, concat_axis=0, tiled=True)]
    all_to_all x1 -> x0, starting transfers between devices: 11 us -> none  [summed_on_arrival(): lax.all_to_all(tiles, axis, split_axis=0, concat_axis=0, tiled=True)]
    all_gather x1 -> x0, blocking collectives: 9.71 us -> none  [gathered_by_axis(): x = lax.all_gather(x, axis, axis=dim, tiled=True)]
    dot_general x11 -> x0, matrix products: 6.63 us -> none  [the longest x1 1.26 us: local(): key_part = jnp.dot(scaled, w_key, preferred_element_type=jnp.float32)]
    ppermute x1 -> x0, starting transfers between devices: 5.14 us -> none  [swapped(): lax.ppermute(x, axis, [(i, i ^ 1 << bit) for i in range(lax.axis_size(axi...]
  transfers between devices with their start and end apart: 3 -> 0, of which waited for: 2 -> 0; matrix products, arithmetic and copies ran while one was open for 1% -> 0% of each run, Pallas kernels for 0% -> 0%
where the time goes in v1:
time: 75.8 us; the launch traced here: 75.7 us
  Pallas kernels  75 us (99%)
    pallas_call x1, Pallas kernels, local(): pl.pallas_call(functools.partial(layer, nz, ny), out_shape=tuple((vm(*x)...  74 us

profile of v1, /device:TPU:1, one launch (start us, length us, event | category | flops | bytes accessed | tf_op | source)
XLA Modules:
  0.0 75.7 jit_solution(3108354603871855801)
XLA Ops:
  0.6 74.0 %shard_map.192 = (bf16[32,128]{1,0:T(8,128)(2,1)S(1)}, f32[16,128,128]{2,1,0:T(8,128)S(1)}, f32[16,128]{1,0:T(8,128)S(1)}, f32[2,8]{1,0:T(2,128)S(1)}) custom-call(bf16[64,128]{1,0:T(8,128)(2,1)} %bitcast.19, f32[1,64]{1,0:T(1,128)} %bitcast.24, bf16[64,1024]{1,0:T(8,128)(2,1)} %wq_hbm.1, bf16[64,1024]{1,0:T(8,128)(2,1)} %wk_hbm.1, bf16[64,1024]{1,0:T(8,128)(2,1)} %wv_hbm.1, ...), custom_call_target="tpu_custom_call" | custom-call | tf_op jit(solution)/shard_map/pallas_call | solution.py:763
  74.6 1.0 %shard_map.193 = (bf16[32,128]{1,0:T(8,128)(2,1)}, f32[16,128,128]{2,1,0:T(8,128)}, f32[16,128]{1,0:T(8,128)}, f32[2,8]{1,0:T(2,128)}) custom-call(bf16[32,128]{1,0:T(8,128)(2,1)S(1)} %get-tuple-element.12.mixed, f32[16,128,128]{2,1,0:T(8,128)S(1)} %get-tuple-element.13.memory, f32[16,128]{1,0:T(8,128)S(1)} %get-tuple-element.14.norm, ...), custom_call_target="tpu_custom_call" | custom-call | tf_op jit(solution)/shard_map/pallas_call | solution.py:773

commit v2 on v1

--- a/solution.py
+++ b/solution.py
@@ -103,6 +103,7 @@
     esend,
     erelay,
     erecv,
+    here_sem,
     loc_sem,
     pair_send,
     pair_recv,
@@ -186,11 +187,8 @@
 
     barrier = pltpu.get_barrier_semaphore()
 
-    def greet(d, _):
+    for d in (1, nz - 1):
         pl.semaphore_signal(barrier, inc=1, device_id={"kv_0": zpeer(d)}, device_id_type=MESH)
-        return 0
-
-    lax.fori_loop(1, nz, greet, 0)
     for d in range(1, ny):
         pl.semaphore_signal(barrier, inc=1, device_id={"kv_1": ypeer(d)}, device_id_type=MESH)
     pl.semaphore_signal(barrier, inc=1, device_id={"tp": other}, device_id_type=MESH)
@@ -245,6 +243,17 @@
             ysend.at[g, ypeer(d)], yrecv.at[g, d - 1], y1_send.at[0], y1_recv.at[g], "kv_1", ypeer(d)
         )
 
+    rounds = [2**k for k in range(nz.bit_length() - 2)]
+
+    def tell(k):
+        for d in (rounds[k], nz - rounds[k]):
+            pl.semaphore_signal(here_sem.at[k], inc=1, device_id={"kv_0": zpeer(d)}, device_id_type=MESH)
+
+    def told(k):
+        pl.semaphore_wait(here_sem.at[k], 2)
+        if k + 1 < len(rounds):
+            tell(k + 1)
+
     pltpu.make_async_copy(wqkv, wqkv, loc_sem.at[4]).wait()
     for g in range(groups):
         part = slice(g * ny * grow, (g + 1) * ny * grow)
@@ -258,7 +267,8 @@
             for to in range(ny):
                 ysend[g, to, :, at : at + values.shape[1]] = values[to * grow : (to + 1) * grow].astype(bf16)
         if g == 0:
-            pl.semaphore_wait(barrier, (nz - 1) + (ny - 1) + 1)
+            pl.semaphore_wait(barrier, 2 + (ny - 1) + 1)
+            tell(0)
         for d in far_first:
             y1(g, d).start()
 
@@ -278,6 +288,9 @@
     for op in pair:
         op.start()
 
+    for k in range(len(rounds) - 1):
+        told(k)
+
     memory.wait()
 
     def split_memory(i, _):
@@ -318,6 +331,8 @@
                     at = g * per * zrow + (k // 8) * 16 + b * 8 + k % 8
                     tq[pl.ds(at, per, stride=zrow), :] = total[b * per : (b + 1) * per]
             else:
+                if g == 0:
+                    told(len(rounds) - 1)
                 total = total + pltpu.roll(total, 64, 1)
                 lane = lax.broadcasted_iota(jnp.int32, (1, HD), 1)
                 for i in range(per):
@@ -732,6 +747,7 @@
         vm((nz, own_cols, rows), bf16),
         vm((nz, own_cols, rows), bf16),
         vm((nz, own_cols, rows), bf16),
+        pltpu.SemaphoreType.REGULAR((nz.bit_length() - 2,)),
         dma((14,)),
         dma((4,)),
         dma((4,)),

time: 75.8 us -> 73.8 us (0.974)
  Pallas kernels: 75 us -> 73 us
    pallas_call x1, Pallas kernels: 74 us -> 72 us  [local(): pl.pallas_call(functools.partial(layer, nz, ny), out_shape=tuple((vm(*x)...]
where the time goes in v2:
time: 73.8 us; the launch traced here: 73.6 us
  Pallas kernels  73 us (99%)
    pallas_call x1, Pallas kernels, local(): pl.pallas_call(functools.partial(layer, nz, ny), out_shape=tuple((vm(*x)...  72 us

profile of v2, /device:TPU:1, one launch (start us, length us, event | category | flops | bytes accessed | tf_op | source)
XLA Modules:
  0.0 73.6 jit_solution(14892277930536346950)
XLA Ops:
  0.6 72.0 %shard_map.192 = (bf16[32,128]{1,0:T(8,128)(2,1)S(1)}, f32[16,128,128]{2,1,0:T(8,128)S(1)}, f32[16,128]{1,0:T(8,128)S(1)}, f32[2,8]{1,0:T(2,128)S(1)}) custom-call(bf16[64,128]{1,0:T(8,128)(2,1)} %bitcast.19, f32[1,64]{1,0:T(1,128)} %bitcast.24, bf16[64,1024]{1,0:T(8,128)(2,1)} %wq_hbm.1, bf16[64,1024]{1,0:T(8,128)(2,1)} %wk_hbm.1, bf16[64,1024]{1,0:T(8,128)(2,1)} %wv_hbm.1, ...), custom_call_target="tpu_custom_call" | custom-call | tf_op jit(solution)/shard_map/pallas_call | solution.py:779
  72.6 1.0 %shard_map.193 = (bf16[32,128]{1,0:T(8,128)(2,1)}, f32[16,128,128]{2,1,0:T(8,128)}, f32[16,128]{1,0:T(8,128)}, f32[2,8]{1,0:T(2,128)}) custom-call(bf16[32,128]{1,0:T(8,128)(2,1)S(1)} %get-tuple-element.12.mixed, f32[16,128,128]{2,1,0:T(8,128)S(1)} %get-tuple-element.13.memory, f32[16,128]{1,0:T(8,128)S(1)} %get-tuple-element.14.norm, ...), custom_call_target="tpu_custom_call" | custom-call | tf_op jit(solution)/shard_map/pallas_call | solution.py:789

commit v3 on v2

--- a/solution.py
+++ b/solution.py
@@ -197,7 +197,7 @@
 
     for op in first[:4]:
         op.wait()
-    groups = dsend.shape[1]
+    groups = ysend.shape[0]
     per = nz // groups
     grow = 2 * per
     order = ORDER[nz]
@@ -371,13 +371,18 @@
     down.wait()
     pair[0].wait_recv()
 
-    def turn(i, _):
-        part = pl.ds(pl.multiple_of(i * HD, 128), HD)
+    mine_cols = ny * own_cols
+    k = lax.broadcasted_iota(jnp.int32, (mine_cols, chunk), 0)
+    at = lax.broadcasted_iota(jnp.int32, (mine_cols, chunk), 1)
+    pick = jnp.where(at == (k // own_cols) * cols + c * own_cols + k % own_cols, 1.0, 0.0).astype(bf16)
+
+    def turn(m, _):
+        part = pl.ds(pl.multiple_of(m * chunk, 128), chunk)
         for t in range(2):
-            wdt[t, pl.ds(pl.multiple_of(i * HD, 128), HD), :] = wdraw[t, :, part].astype(f32).T.astype(bf16)
+            wdt[t, m] = dot(pick, wdraw[t, :, part], NT).astype(bf16)
         return 0
 
-    lax.fori_loop(0, model // HD, turn, 0)
+    lax.fori_loop(0, nz, turn, 0)
 
     for op in small:
         op.wait()
@@ -506,7 +511,7 @@
 
     @pl.when(mine)
     def _():
-        for o in odds:
+        for o in reversed(odds):
             z3(o).start()
         for d in far_first:
             y3_own(d).start()
@@ -540,7 +545,7 @@
         square = jnp.sum((wide * wide).reshape(ny * cols // 8, 8, rows), axis=0)
         xsend[4 * fpad : 4 * fpad + 8, :] += square
 
-    lag = min(3, hz)
+    lag = hz
     xsend[...] = jnp.zeros_like(xsend)
 
     def forward_z3(k):
@@ -589,28 +594,32 @@
         gate, up = units(2 * t), units(2 * t + 1)
         active.append((gate / (1.0 + jnp.exp(-gate)) * up).astype(bf16))
 
+    groups, per = dsend.shape[1], nz // dsend.shape[1]
+
     def y5(d, g):
         return rcopy(dsend.at[ypeer(d), g], drecv.at[g, d - 1], y5_send.at[0], y5_recv.at[g], "kv_1", ypeer(d))
 
     def place5(k):
         return zpeer(order[k])
 
-    def produce(to, g):
-        total = jnp.zeros((per * own_cols, rows), f32)
+    def produce(targets):
+        parts = []
+        for to, g in targets:
+            part = pl.ds(pl.multiple_of(to * own_cols, own_cols), own_cols)
+            parts += [(place5(g * per + i), part) for i in range(per)]
+        total = 0.0
         for t in range(2):
-            parts = [
-                wdt[t, pl.ds(pl.multiple_of((place5(g * per + i) * ny + to) * cols + c * own_cols, own_cols), own_cols), :]
-                for i in range(per)
-            ]
-            total = total + dot(jnp.concatenate(parts, axis=0), active[t], NN)
-        dsend[to, g] = total.astype(bf16)
+            left = jnp.concatenate([wdt[t, place, part, :] for place, part in parts], axis=0)
+            total = total + dot(left, active[t], NN)
+        size = per * own_cols
+        for n, (to, g) in enumerate(targets):
+            dsend[to, g] = total[n * size : (n + 1) * size].astype(bf16)
 
     for g in range(groups):
+        produce([(ypeer(d), g) for d in far_first])
         for d in far_first:
-            produce(ypeer(d), g)
             y5(d, g).start()
-    for g in range(groups):
-        produce(y, g)
+    produce([(y, g) for g in range(groups)])
 
     def z5(o):
         return onward(o, esend, erelay, erecv, z5_send.at[0], z5_relay, z5_recv.at[0])
@@ -681,7 +690,7 @@
     width = heads * HD
     total = HD + 3 * width
     own_cols = cols // 2
-    groups = min(4, nz)
+    groups, groups5 = min(4, nz), min(8, nz)
     per = nz // groups
     hz = nz // 2
     zrow = 6 * heads
@@ -724,7 +733,7 @@
         vm((4, ff, model // 2), bf16),
         vm((4 * fpad, model // 2), bf16),
         vm((2, ff, model), bf16),
-        vm((2, model, ff), bf16),
+        vm((2, nz, ny * own_cols, ff), bf16),
         vm((2 * heads, HD, 2 * HD), bf16),
         vm((groups, ny, 2 * per, total), bf16),
         vm((groups, ny - 1, 2 * per, total), bf16),
@@ -742,8 +751,8 @@
         vm((hz, ny, cols, rows), bf16),
         vm((4 * fpad + 8, rows), f32),
         vm((4 * fpad + 8, rows), f32),
-        vm((ny, groups, per * own_cols, rows), bf16),
-        vm((groups, ny - 1, per * own_cols, rows), bf16),
+        vm((ny, groups5, nz // groups5 * own_cols, rows), bf16),
+        vm((groups5, ny - 1, nz // groups5 * own_cols, rows), bf16),
         vm((nz, own_cols, rows), bf16),
         vm((nz, own_cols, rows), bf16),
         vm((nz, own_cols, rows), bf16),
@@ -765,7 +774,7 @@
         dma((1,)),
         dma((hz,)),
         dma((1,)),
-        dma((groups,)),
+        dma((groups5,)),
         dma((1,)),
         dma((joins,)),
         dma((1,)),

time: 73.8 us -> 71.1 us (0.963)
  Pallas kernels: 73 us -> 70.2 us
    pallas_call x1, Pallas kernels: 72 us -> 69.2 us  [local(): pl.pallas_call(functools.partial(layer, nz, ny), out_shape=tuple((vm(*x)...]
where the time goes in v3:
time: 71.1 us; the launch traced here: 70.9 us
  Pallas kernels  70.2 us (99%)
    pallas_call x1, Pallas kernels, local(): pl.pallas_call(functools.partial(layer, nz, ny), out_shape=tuple((vm(*x)...  69.2 us

profile of v3, /device:TPU:1, one launch (start us, length us, event | category | flops | bytes accessed | tf_op | source)
XLA Modules:
  0.0 70.9 jit_solution(8971810206325785180)
XLA Ops:
  0.6 69.2 %shard_map.192 = (bf16[32,128]{1,0:T(8,128)(2,1)S(1)}, f32[16,128,128]{2,1,0:T(8,128)S(1)}, f32[16,128]{1,0:T(8,128)S(1)}, f32[2,8]{1,0:T(2,128)S(1)}) custom-call(bf16[64,128]{1,0:T(8,128)(2,1)} %bitcast.19, f32[1,64]{1,0:T(1,128)} %bitcast.24, bf16[64,1024]{1,0:T(8,128)(2,1)} %wq_hbm.1, bf16[64,1024]{1,0:T(8,128)(2,1)} %wk_hbm.1, bf16[64,1024]{1,0:T(8,128)(2,1)} %wv_hbm.1, ...), custom_call_target="tpu_custom_call" | custom-call | tf_op jit(solution)/shard_map/pallas_call | solution.py:788
  69.9 1.0 %shard_map.193 = (bf16[32,128]{1,0:T(8,128)(2,1)}, f32[16,128,128]{2,1,0:T(8,128)}, f32[16,128]{1,0:T(8,128)}, f32[2,8]{1,0:T(2,128)}) custom-call(bf16[32,128]{1,0:T(8,128)(2,1)S(1)} %get-tuple-element.12.mixed, f32[16,128,128]{2,1,0:T(8,128)S(1)} %get-tuple-element.13.memory, f32[16,128]{1,0:T(8,128)S(1)} %get-tuple-element.14.norm, ...), custom_call_target="tpu_custom_call" | custom-call | tf_op jit(solution)/shard_map/pallas_call | solution.py:798

commit v4 on v3

--- a/solution.py
+++ b/solution.py
@@ -90,6 +90,7 @@
     zrecv,
     zgsend,
     zgrecv,
+    hidx,
     hidg,
     hidf,
     bsend,
@@ -147,8 +148,9 @@
         return lax.rem(y + d, ny)
 
     def rcopy(src, dst, ssem, rsem, axis, to):
+        place = to if axis is None else {axis: to}
         return pltpu.make_async_remote_copy(
-            src_ref=src, dst_ref=dst, send_sem=ssem, recv_sem=rsem, device_id={axis: to}, device_id_type=MESH
+            src_ref=src, dst_ref=dst, send_sem=ssem, recv_sem=rsem, device_id=place, device_id_type=MESH
         )
 
     def local(src, dst, k):
@@ -156,8 +158,10 @@
 
     chunk = ny * cols
 
-    def from_z(m, core):
-        return pl.ds(pl.multiple_of((2 * m + core) * chunk, 128), chunk)
+    parity = lax.rem(z + 1 + c, 2)
+
+    def from_z(m, side):
+        return pl.ds(pl.multiple_of((2 * m + side) * chunk, 128), chunk)
 
     def place(m):
         return pl.ds(m * chunk, chunk)
@@ -176,9 +180,9 @@
     late = []
     for m in range(hz):
         late += [
-            local(gmlp_hbm.at[:, from_z(m, c)], gmlp.at[:, place(m)], 10),
-            local(wg_hbm.at[:, from_z(m, c)], wraw.at[2 * c, :, place(m)], 11),
-            local(wu_hbm.at[:, from_z(m, c)], wraw.at[2 * c + 1, :, place(m)], 11),
+            local(gmlp_hbm.at[:, from_z(m, parity)], gmlp.at[:, place(m)], 10),
+            local(wg_hbm.at[:, from_z(m, parity)], wraw.at[2 * c, :, place(m)], 11),
+            local(wu_hbm.at[:, from_z(m, parity)], wraw.at[2 * c + 1, :, place(m)], 11),
         ]
     down = local(wd_hbm, wdraw.at[c], 12)
     output = local(wo_hbm, wo, 13)
@@ -277,7 +281,7 @@
         for k, w_hbm in enumerate((wg_hbm, wu_hbm)):
             pair.append(
                 rcopy(
-                    w_hbm.at[:, from_z(m, other)],
+                    w_hbm.at[:, from_z(m, 1 - parity)],
                     wraw.at[2 * c + k, :, place(m)],
                     pair_send.at[0],
                     pair_recv.at[0],
@@ -447,15 +451,20 @@
     hidg[me] = hidden.astype(bf16)
 
     def z2(d):
-        return rcopy(hidg.at[me], hidg.at[me], z2_send.at[0], z2_recv.at[d], "kv_0", zpeer(d))
+        place = {"kv_0": zpeer(d), "tp": other}
+        return rcopy(hidg.at[me], hidx.at[z], z2_send.at[0], z2_recv.at[d], None, place)
 
     def z2_in(d):
-        j = lax.rem(z + nz - d, nz) * ny + y
-        return rcopy(hidg.at[j], hidg.at[j], z2_send.at[0], z2_recv.at[d], "kv_0", zpeer(d))
+        at = hidx.at[lax.rem(z + nz - d, nz)]
+        return rcopy(at, at, z2_send.at[0], z2_recv.at[d], "kv_0", zpeer(d))
+
+    def y2_own(d):
+        return rcopy(hidg.at[me], hidg.at[me], y2_send.at[0], y2_recv.at[0], "kv_1", ypeer(d))
 
     def y2(d, dz):
-        j = lax.rem(z + nz - dz, nz) * ny + y
-        return rcopy(hidg.at[j], hidg.at[j], y2_send.at[0], y2_recv.at[0], "kv_1", ypeer(d))
+        source = lax.rem(z + nz - dz, nz)
+        place = {"kv_1": ypeer(d), "tp": other} if d else {"tp": other}
+        return rcopy(hidx.at[source], hidg.at[source * ny + y], y2_send.at[0], y2_recv.at[0], None, place)
 
     def start_z2(i, _):
         z2(near_first(nz - 2 - i, nz)).start()
@@ -463,7 +472,7 @@
 
     lax.fori_loop(0, nz - 1, start_z2, 0)
     for d in far_first:
-        y2(d, 0).start()
+        y2_own(d).start()
 
     norm_ref[...] = norm_next
     stab_ref[...] = jnp.concatenate(
@@ -476,14 +485,14 @@
     def forward_z2(i, _):
         dz = near_first(i, nz)
         z2_in(dz).wait_recv()
-        for d in far_first:
+        for d in far_first + [0]:
             y2(d, dz).start()
         return 0
 
     lax.fori_loop(0, nz - 1, forward_z2, 0)
     output.wait()
 
-    together(hidg.at[pl.ds(0, (ny - 1) * nz)], y2_recv.at[0]).wait()
+    together(hidg.at[pl.ds(0, nkv - 1)], y2_recv.at[0]).wait()
     hidf[...] = hidg[...].astype(f32).reshape(nkv * 16, HD)
     branch = jnp.zeros((cols, rows), f32)
     for h in range(8):
@@ -497,11 +506,11 @@
     res[...] = residual
 
     zz = z // 2
-    odd = lax.rem(z + c, 2)
+    odd = 1 - c
     mine = odd == 0
 
     def z3(d):
-        return rcopy(res, resg.at[zz, y], z3_send.at[0], z3_recv.at[d], "kv_0", zpeer(d))
+        return rcopy(res, resg.at[zz, y], z3_send.at[0], z3_recv.at[d], None, {"kv_0": zpeer(d), "tp": 0})
 
     def y3_own(d):
         return rcopy(res, resg.at[zz, y], y3_send.at[0], y3_recv.at[zz], "kv_1", ypeer(d))
@@ -534,7 +543,8 @@
         at = resg.at[source3(k) // 2, y]
         step = 1 - 2 * lax.rem(k, 2)
         d = offset3(k) + step
-        return rcopy(at, at, z3_send.at[0], z3_recv.at[d], "kv_0", lax.rem(z + nz + step, nz))
+        place = {"kv_0": lax.rem(z + nz + step, nz), "tp": 1}
+        return rcopy(at, at, z3_send.at[0], z3_recv.at[d], None, place)
 
     def accumulate(i):
         together(resg.at[i, pl.ds(0, ny - 1)], y3_recv.at[i]).wait()
@@ -655,7 +665,7 @@
     together(zsend.at[pl.ds(1, nz - 1)], z1_send.at[0]).wait()
     together(zgsend.at[pl.ds(1, nz - 1)], z1_send.at[1]).wait()
     together(hidg.at[pl.ds(0, nz - 1)], z2_send.at[0]).wait()
-    together(hidg.at[pl.ds(0, (ny - 1) * nz)], y2_send.at[0]).wait()
+    together(hidg.at[pl.ds(0, nkv - 1)], y2_send.at[0]).wait()
     together(drecv, y5_send.at[0]).wait()
     together(esend.at[pl.ds(1, nz - 1)], z5_send.at[0]).wait()
     together(resg.at[:, pl.ds(0, ny - 1)], y3_send.at[0]).wait()
@@ -743,6 +753,7 @@
         vm((nz, zrow, HD), bf16),
         vm((nz, 1, HD), f32),
         vm((nz, 1, HD), f32),
+        vm((nz, 2 * heads, HD), bf16),
         vm((nkv, 2 * heads, HD), bf16),
         vm((nkv * 2 * heads, HD), f32),
         vm((cols, rows), bf16),

time: 71.1 us -> 70.1 us (0.986)
  the two profiles are of different devices: /device:TPU:1 before, /device:TPU:4 now
where the time goes in v4:
time: 70.1 us; the launch traced here: 69.9 us
  Pallas kernels  69.3 us (99%)
    pallas_call x1, Pallas kernels, local(): pl.pallas_call(functools.partial(layer, nz, ny), out_shape=tuple((vm(*x)...  68.2 us

profile of v4, /device:TPU:4, one launch (start us, length us, event | category | flops | bytes accessed | tf_op | source)
XLA Modules:
  0.0 69.9 jit_solution(16402583696199703634)
XLA Ops:
  0.6 68.2 %shard_map.192 = (bf16[32,128]{1,0:T(8,128)(2,1)S(1)}, f32[16,128,128]{2,1,0:T(8,128)S(1)}, f32[16,128]{1,0:T(8,128)S(1)}, f32[2,8]{1,0:T(2,128)S(1)}) custom-call(bf16[64,128]{1,0:T(8,128)(2,1)} %bitcast.19, f32[1,64]{1,0:T(1,128)} %bitcast.24, bf16[64,1024]{1,0:T(8,128)(2,1)} %wq_hbm.1, bf16[64,1024]{1,0:T(8,128)(2,1)} %wk_hbm.1, bf16[64,1024]{1,0:T(8,128)(2,1)} %wv_hbm.1, ...), custom_call_target="tpu_custom_call" | custom-call | tf_op jit(solution)/shard_map/pallas_call | solution.py:799
  68.9 1.0 %shard_map.193 = (bf16[32,128]{1,0:T(8,128)(2,1)}, f32[16,128,128]{2,1,0:T(8,128)}, f32[16,128]{1,0:T(8,128)}, f32[2,8]{1,0:T(2,128)}) custom-call(bf16[32,128]{1,0:T(8,128)(2,1)S(1)} %get-tuple-element.12.mixed, f32[16,128,128]{2,1,0:T(8,128)S(1)} %get-tuple-element.13.memory, f32[16,128]{1,0:T(8,128)S(1)} %get-tuple-element.14.norm, ...), custom_call_target="tpu_custom_call" | custom-call | tf_op jit(solution)/shard_map/pallas_call | solution.py:809

commit v5 on v4

--- a/solution.py
+++ b/solution.py
@@ -625,9 +625,10 @@
         for n, (to, g) in enumerate(targets):
             dsend[to, g] = total[n * size : (n + 1) * size].astype(bf16)
 
-    for g in range(groups):
-        produce([(ypeer(d), g) for d in far_first])
-        for d in far_first:
+    for first_g in range(0, groups, 2):
+        both = [(d, g) for g in (first_g, first_g + 1) for d in far_first]
+        produce([(ypeer(d), g) for d, g in both])
+        for d, g in both:
             y5(d, g).start()
     produce([(y, g) for g in range(groups)])
 
@@ -700,7 +701,7 @@
     width = heads * HD
     total = HD + 3 * width
     own_cols = cols // 2
-    groups, groups5 = min(4, nz), min(8, nz)
+    groups, groups5 = min(4, nz), nz
     per = nz // groups
     hz = nz // 2
     zrow = 6 * heads

time: 70.1 us -> 70 us (level)
  no operation moved by 1% of the time
where the time goes in v5:
time: 70 us; the launch traced here: 69.8 us
  Pallas kernels  69.2 us (99%)
    pallas_call x1, Pallas kernels, local(): pl.pallas_call(functools.partial(layer, nz, ny), out_shape=tuple((vm(*x)...  68.1 us

profile of v5, /device:TPU:4, one launch (start us, length us, event | category | flops | bytes accessed | tf_op | source)
XLA Modules:
  0.0 69.8 jit_solution(15266156514244162291)
XLA Ops:
  0.6 68.1 %shard_map.192 = (bf16[32,128]{1,0:T(8,128)(2,1)S(1)}, f32[16,128,128]{2,1,0:T(8,128)S(1)}, f32[16,128]{1,0:T(8,128)S(1)}, f32[2,8]{1,0:T(2,128)S(1)}) custom-call(bf16[64,128]{1,0:T(8,128)(2,1)} %bitcast.19, f32[1,64]{1,0:T(1,128)} %bitcast.24, bf16[64,1024]{1,0:T(8,128)(2,1)} %wq_hbm.1, bf16[64,1024]{1,0:T(8,128)(2,1)} %wk_hbm.1, bf16[64,1024]{1,0:T(8,128)(2,1)} %wv_hbm.1, ...), custom_call_target="tpu_custom_call" | custom-call | tf_op jit(solution)/shard_map/pallas_call | solution.py:800
  68.8 1.0 %shard_map.193 = (bf16[32,128]{1,0:T(8,128)(2,1)}, f32[16,128,128]{2,1,0:T(8,128)}, f32[16,128]{1,0:T(8,128)}, f32[2,8]{1,0:T(2,128)}) custom-call(bf16[32,128]{1,0:T(8,128)(2,1)S(1)} %get-tuple-element.12.mixed, f32[16,128,128]{2,1,0:T(8,128)S(1)} %get-tuple-element.13.memory, f32[16,128]{1,0:T(8,128)S(1)} %get-tuple-element.14.norm, ...), custom_call_target="tpu_custom_call" | custom-call | tf_op jit(solution)/shard_map/pallas_call | solution.py:810
